TPU v7x, 32 devices: a whole 2x2x4 slice. The times are simulated.
32 devices in a mesh: sp: 8 (over z, y), tp: 4 (over x, core).
Axes of the slice: x: 2, y: 2, z: 4, core: 2. Of those that a mesh axis runs over, the one named last changes fastest.
Arguments:
- resid: bfloat16 [2048, 2048], P(('sp', 'tp')), may hold values from -6 to 6
- mix_in: bfloat16 [2048, 512], P('sp', 'tp'), may hold values from -6 to 6
- decay_rate: float32 [32, 64], P('tp'), may hold values from -0.05 to 0, as said below
- turn_rate: float32 [32, 64], P('tp'), may hold values from -3.140625 to 3.140625
- forget: float32 [2048, 32], P('sp', 'tp'), may hold values from -2 to 0, as said below
- input_real: float32 [32, 64, 16], P('tp'), may hold values from -1 to 1
- input_imag: float32 [32, 64, 16], P('tp'), may hold values from -1 to 1
- output_real: float32 [32, 16, 64], P('tp'), may hold values from -0.75 to 0.75
- output_imag: float32 [32, 16, 64], P('tp'), may hold values from -0.75 to 0.75
- skip_gain: float32 [32, 16], P('tp'), may hold values from -5 to 5
- mix_gain: float32 [512], replicated, may hold values from 0.1 to 1.9
- w_out: bfloat16 [512, 2048], replicated, may hold values from -0.25 to 0.25
- ffn_gain: float32 [2048], replicated, may hold values from 0.1 to 1.9
- gating_matrix: bfloat16 [2048, 5632], P('sp', 'tp'), may hold values from -0.125 to 0.125
- w_up: bfloat16 [2048, 5632], P('sp', 'tp'), may hold values from -0.125 to 0.125
- w_down: bfloat16 [5632, 2048], P('tp', 'sp'), may hold values from -0.078125 to 0.078125
Outputs:
- result: bfloat16 [2048, 2048], P(('sp', 'tp'))
Inputs may be any that keep to these rules, and one draw needn't show every extreme that they name: `decay_rate`: every entry is negative. `forget`: every entry is at most zero.
All inputs are finite; a program needn't handle non-finite values.
Results may differ from a plain program's by a relative error of at most 0.012.
Values may be sent and summed in bfloat16 or wider, within the bound.
A program may use at most 128 MiB of HBM per device.

v0:
```python
import jax
import jax.numpy as jnp
from jax import lax
from jax.sharding import PartitionSpec as P

eps = 1e-06


def carried_in(part, axis, combine, identity):
    place = lax.axis_index(axis)
    gathered = jax.tree.map(lambda a: lax.all_gather(a, axis), part)
    state = jax.tree.map(lambda a, e: jnp.zeros_like(a) + jnp.asarray(e, a.dtype), part, identity)

    def one(turn, state):
        return combine(
            state, jax.tree.map(lambda a: lax.dynamic_index_in_dim(a, turn, 0, False), gathered)
        )

    return lax.fori_loop(0, place, one, state)


def chain(earlier, later):
    first_real, first_imag, push_real, push_imag = earlier
    next_real, next_imag, add_real, add_imag = later
    return (
        next_real * first_real - next_imag * first_imag,
        next_real * first_imag + next_imag * first_real,
        next_real * push_real - next_imag * push_imag + add_real,
        next_real * push_imag + next_imag * push_real + add_imag,
    )


def local_states(log_step, push_real, push_imag, turn):
    high = lax.Precision.HIGHEST
    n_rows, columns = log_step.shape
    span = min(32, n_rows)
    n_spans = n_rows // span
    place = jnp.arange(span, dtype=jnp.float32)
    lower = place[:, None] >= place[None, :]
    lower_cube = lower[:, :, None]
    triangle = lower.astype(jnp.float32)
    lag_angle = (place[:, None] - place[None, :])[:, :, None] * turn[None, None, :]
    lag_cos = jnp.where(lower_cube, jnp.cos(lag_angle), 0.0)
    lag_sin = jnp.where(lower_cube, jnp.sin(lag_angle), 0.0)
    ahead = place + 1.0
    own_cos = jnp.cos(ahead[:, None] * turn[None, :])
    own_sin = jnp.sin(ahead[:, None] * turn[None, :])

    def advance(carry, blocks):
        run_log, state_real, state_imag, offset = carry
        log_block, real_block, imag_block = blocks
        inner = jnp.dot(triangle, log_block, precision=high)
        spread = jnp.where(lower_cube, inner[:, None, :] - inner[None, :, :], 0.0)
        weight = jnp.where(lower_cube, jnp.exp(spread), 0.0)
        weight_real = weight * lag_cos
        weight_imag = weight * lag_sin
        new_real = jnp.sum(weight_real * real_block[None] - weight_imag * imag_block[None], axis=1)
        new_imag = jnp.sum(weight_real * imag_block[None] + weight_imag * real_block[None], axis=1)
        fade = jnp.exp(inner)
        carry_real = fade * own_cos
        carry_imag = fade * own_sin
        new_real = new_real + carry_real * state_real[None] - carry_imag * state_imag[None]
        new_imag = new_imag + carry_real * state_imag[None] + carry_imag * state_real[None]
        whole_fade = jnp.exp(run_log[None] + inner)
        whole_angle = (offset + ahead)[:, None] * turn[None, :]
        prefix_real = whole_fade * jnp.cos(whole_angle)
        prefix_imag = whole_fade * jnp.sin(whole_angle)
        following = (run_log + inner[-1], new_real[-1], new_imag[-1], offset + span)
        return (following, (new_real, new_imag, prefix_real, prefix_imag))

    zero_row = jnp.zeros((columns,), jnp.float32)
    start = (zero_row, zero_row, zero_row, jnp.zeros((), jnp.float32))
    blocks = (
        log_step.reshape(n_spans, span, columns),
        push_real.reshape(n_spans, span, columns),
        push_imag.reshape(n_spans, span, columns),
    )
    final, outputs = lax.scan(advance, start, blocks)
    outputs = tuple((item.reshape(n_rows, columns) for item in outputs))
    total_fade = jnp.exp(final[0])
    totals = (
        total_fade * jnp.cos(n_rows * turn),
        total_fade * jnp.sin(n_rows * turn),
        final[1],
        final[2],
    )
    return (outputs, totals)


def per_device(
    resid,
    mix_in,
    decay_rate,
    turn_rate,
    forget,
    input_real,
    input_imag,
    output_real,
    output_imag,
    skip_gain,
    mix_gain,
    w_out,
    ffn_gain,
    gating_matrix,
    w_up,
    w_down,
):
    high = lax.Precision.HIGHEST
    n_rows, local_width = mix_in.shape
    n_groups, n_state = decay_rate.shape
    n_chan = input_real.shape[2]
    drive = mix_in.astype(jnp.float32).reshape(n_rows, n_groups, n_chan)
    in_factor = jnp.sqrt(-jnp.expm1(2.0 * decay_rate))
    push_real = jnp.einsum(
        "gph,tgh->tgp", input_real * in_factor[:, :, None], drive, precision=high
    ).reshape(n_rows, n_groups * n_state)
    push_imag = jnp.einsum(
        "gph,tgh->tgp", input_imag * in_factor[:, :, None], drive, precision=high
    ).reshape(n_rows, n_groups * n_state)
    log_step = (decay_rate[None] + forget[:, :, None]).reshape(n_rows, n_groups * n_state)
    turn = turn_rate.reshape(n_groups * n_state)
    outputs, totals = local_states(log_step, push_real, push_imag, turn)
    inner_real, inner_imag, prefix_real, prefix_imag = outputs
    ones_row = jnp.ones((n_groups * n_state,), jnp.float32)
    zeroed_row = jnp.zeros((n_groups * n_state,), jnp.float32)
    carry_in = carried_in(totals, "sp", chain, (ones_row, zeroed_row, zeroed_row, zeroed_row))
    state_real = inner_real + prefix_real * carry_in[2][None] - prefix_imag * carry_in[3][None]
    state_imag = inner_imag + prefix_real * carry_in[3][None] + prefix_imag * carry_in[2][None]
    response = (
        jnp.einsum(
            "ghp,tgp->tgh",
            output_real,
            state_real.reshape(n_rows, n_groups, n_state),
            precision=high,
        )
        - jnp.einsum(
            "ghp,tgp->tgh",
            output_imag,
            state_imag.reshape(n_rows, n_groups, n_state),
            precision=high,
        )
        + skip_gain[None] * drive
    )
    mixer_out = jax.nn.gelu(response.reshape(n_rows, local_width)).astype(jnp.bfloat16)
    swapped = lax.all_to_all(mixer_out, "tp", split_axis=0, concat_axis=1, tiled=True)
    mixed_f = swapped.astype(jnp.float32)
    normed = (
        mixed_f * lax.rsqrt(jnp.mean(mixed_f * mixed_f, axis=1, keepdims=True) + eps) * mix_gain
    ).astype(jnp.bfloat16)
    projected = jnp.dot(normed, w_out, preferred_element_type=jnp.float32)
    resid_mid = resid.astype(jnp.float32) + projected
    ffn_in = (
        resid_mid
        * lax.rsqrt(jnp.mean(resid_mid * resid_mid, axis=1, keepdims=True) + eps)
        * ffn_gain
    ).astype(jnp.bfloat16)
    gathered = lax.all_gather(ffn_in, "tp", axis=0, tiled=True)
    gate_val = jnp.dot(
        gathered,
        lax.all_gather(gating_matrix, "sp", axis=0, tiled=True),
        preferred_element_type=jnp.float32,
    )
    up_val = jnp.dot(
        gathered, lax.all_gather(w_up, "sp", axis=0, tiled=True), preferred_element_type=jnp.float32
    )
    hidden = (jax.nn.silu(gate_val) * up_val).astype(jnp.bfloat16)
    partial_value = jnp.dot(
        hidden, lax.all_gather(w_down, "sp", axis=1, tiled=True), preferred_element_type=jnp.float32
    )
    ffn = lax.psum_scatter(
        partial_value.astype(jnp.bfloat16), "tp", scatter_dimension=0, tiled=True
    ).astype(jnp.float32)
    return (resid_mid + 0.5 * ffn).astype(jnp.bfloat16)


def solution(mesh):
    placed = (
        P(("sp", "tp"), None),
        P("sp", "tp"),
        P("tp", None),
        P("tp", None),
        P("sp", "tp"),
        P("tp", None, None),
        P("tp", None, None),
        P("tp", None, None),
        P("tp", None, None),
        P("tp", None),
        P(),
        P(),
        P(),
        P("sp", "tp"),
        P("sp", "tp"),
        P("tp", "sp"),
    )
    return jax.shard_map(
        per_device, mesh=mesh, in_specs=placed, out_specs=P(("sp", "tp"), None), check_vma=False
    )
```

profile of v0, /device:TPU:0, one launch (start us, length us, event | category | flops | bytes accessed | tf_op | source)
XLA Modules:
  0.0 576.9 jit_solution(734002597552785004)
XLA Ops:
  10.7 2.1 convolution_bitcast_fusion.2
  12.8 1.5 copy.52
  16.5 1.5 copy.53
  21.7 93.2 %while.45 = (s32[]{:T(128)}, f32[512]{0:T(512)S(1)}, f32[512]{0:T(512)S(1)}, f32[512]{0:T(512)S(1)}, f32[]{:T(128)}, /*index=5*/f32[8,32,512]{2,1,0:T(8,128)}, f...) while((s32[]{:T(128)}, f32[512]{0:T(512)S(1)}, ...), condition=%wide.wide.region_3.4_spmd.clone.clone.clone.clone, body=%wide.wide.region_0.3_spmd.clone.clone.clone.clone.sunk | while | flops 14897220 | bytes 1351775 | solution.py:78
  22.9 9.2 %add_reduce_fusion.3 = (f32[32,512]{1,0:T(8,128)S(1)}, f32[32,512]{1,0:T(8,128)S(1)}) fusion(f32[512]{0:T(512)S(1)} %get-tuple-element.853, f32[32,32]{1,0:T(8,128)S(1)} %get-tuple-element.854, f32[32,512]{1,0:T(8,128)S(1)} %get-tuple-element.788, f32[32,512]{1,0:T(8,128)S(1)} %get-tuple-element.789, ...), kind=kLoop, calls=%fused_computation.19.clone.clone.1 | loop fusion | flops 8355840 | bytes 335872 | tf_op jit(solution)/shard_map/while/body/eval_jaxpr/reduce_sum | solution.py:58
  34.5 9.2 %add_reduce_fusion.3 = (f32[32,512]{1,0:T(8,128)S(1)}, f32[32,512]{1,0:T(8,128)S(1)}) fusion(f32[512]{0:T(512)S(1)} %get-tuple-element.853, f32[32,32]{1,0:T(8,128)S(1)} %get-tuple-element.854, f32[32,512]{1,0:T(8,128)S(1)} %get-tuple-element.788, f32[32,512]{1,0:T(8,128)S(1)} %get-tuple-element.789, ...), kind=kLoop, calls=%fused_computation.19.clone.clone.1 | loop fusion | flops 8355840 | bytes 335872 | tf_op jit(solution)/shard_map/while/body/eval_jaxpr/reduce_sum | solution.py:58
  46.1 9.2 %add_reduce_fusion.3 = (f32[32,512]{1,0:T(8,128)S(1)}, f32[32,512]{1,0:T(8,128)S(1)}) fusion(f32[512]{0:T(512)S(1)} %get-tuple-element.853, f32[32,32]{1,0:T(8,128)S(1)} %get-tuple-element.854, f32[32,512]{1,0:T(8,128)S(1)} %get-tuple-element.788, f32[32,512]{1,0:T(8,128)S(1)} %get-tuple-element.789, ...), kind=kLoop, calls=%fused_computation.19.clone.clone.1 | loop fusion | flops 8355840 | bytes 335872 | tf_op jit(solution)/shard_map/while/body/eval_jaxpr/reduce_sum | solution.py:58
  57.8 9.2 %add_reduce_fusion.3 = (f32[32,512]{1,0:T(8,128)S(1)}, f32[32,512]{1,0:T(8,128)S(1)}) fusion(f32[512]{0:T(512)S(1)} %get-tuple-element.853, f32[32,32]{1,0:T(8,128)S(1)} %get-tuple-element.854, f32[32,512]{1,0:T(8,128)S(1)} %get-tuple-element.788, f32[32,512]{1,0:T(8,128)S(1)} %get-tuple-element.789, ...), kind=kLoop, calls=%fused_computation.19.clone.clone.1 | loop fusion | flops 8355840 | bytes 335872 | tf_op jit(solution)/shard_map/while/body/eval_jaxpr/reduce_sum | solution.py:58
  69.4 9.2 %add_reduce_fusion.3 = (f32[32,512]{1,0:T(8,128)S(1)}, f32[32,512]{1,0:T(8,128)S(1)}) fusion(f32[512]{0:T(512)S(1)} %get-tuple-element.853, f32[32,32]{1,0:T(8,128)S(1)} %get-tuple-element.854, f32[32,512]{1,0:T(8,128)S(1)} %get-tuple-element.788, f32[32,512]{1,0:T(8,128)S(1)} %get-tuple-element.789, ...), kind=kLoop, calls=%fused_computation.19.clone.clone.1 | loop fusion | flops 8355840 | bytes 335872 | tf_op jit(solution)/shard_map/while/body/eval_jaxpr/reduce_sum | solution.py:58
  78.7 1.3 fusion.82
  81.1 9.2 %add_reduce_fusion.3 = (f32[32,512]{1,0:T(8,128)S(1)}, f32[32,512]{1,0:T(8,128)S(1)}) fusion(f32[512]{0:T(512)S(1)} %get-tuple-element.853, f32[32,32]{1,0:T(8,128)S(1)} %get-tuple-element.854, f32[32,512]{1,0:T(8,128)S(1)} %get-tuple-element.788, f32[32,512]{1,0:T(8,128)S(1)} %get-tuple-element.789, ...), kind=kLoop, calls=%fused_computation.19.clone.clone.1 | loop fusion | flops 8355840 | bytes 335872 | tf_op jit(solution)/shard_map/while/body/eval_jaxpr/reduce_sum | solution.py:58
  90.3 1.2 fusion.82
  92.7 9.2 %add_reduce_fusion.3 = (f32[32,512]{1,0:T(8,128)S(1)}, f32[32,512]{1,0:T(8,128)S(1)}) fusion(f32[512]{0:T(512)S(1)} %get-tuple-element.853, f32[32,32]{1,0:T(8,128)S(1)} %get-tuple-element.854, f32[32,512]{1,0:T(8,128)S(1)} %get-tuple-element.788, f32[32,512]{1,0:T(8,128)S(1)} %get-tuple-element.789, ...), kind=kLoop, calls=%fused_computation.19.clone.clone.1 | loop fusion | flops 8355840 | bytes 335872 | tf_op jit(solution)/shard_map/while/body/eval_jaxpr/reduce_sum | solution.py:58
  102.0 1.2 fusion.82
  104.4 9.2 %add_reduce_fusion.3 = (f32[32,512]{1,0:T(8,128)S(1)}, f32[32,512]{1,0:T(8,128)S(1)}) fusion(f32[512]{0:T(512)S(1)} %get-tuple-element.853, f32[32,32]{1,0:T(8,128)S(1)} %get-tuple-element.854, f32[32,512]{1,0:T(8,128)S(1)} %get-tuple-element.788, f32[32,512]{1,0:T(8,128)S(1)} %get-tuple-element.789, ...), kind=kLoop, calls=%fused_computation.19.clone.clone.1 | loop fusion | flops 8355840 | bytes 335872 | tf_op jit(solution)/shard_map/while/body/eval_jaxpr/reduce_sum | solution.py:58
  114.9 27.9 %all-gather.5 = f32[8,1,512]{2,1,0:T(1,128)S(1)} all-gather(f32[1,1,512]{2,1,0:T(1,128)S(1)} %bitcast.130), channel_id=3, replica_groups=mesh['sp'=8,'tp'=4] {'sp'}, dimensions={0}, use_global_device_ids=true | all-gather | bytes 18432 | tf_op jit(solution)/shard_map/all_gather | solution.py:11
  142.9 26.1 %all-gather.4 = f32[8,1,512]{2,1,0:T(1,128)S(1)} all-gather(f32[1,1,512]{2,1,0:T(1,128)S(1)} %bitcast.129), channel_id=2, replica_groups=mesh['sp'=8,'tp'=4] {'sp'}, dimensions={0}, use_global_device_ids=true | all-gather | bytes 18432 | tf_op jit(solution)/shard_map/all_gather | solution.py:11
  169.0 26.1 %all-gather.7 = f32[8,1,512]{2,1,0:T(1,128)S(1)} all-gather(f32[1,1,512]{2,1,0:T(1,128)S(1)} %bitcast.124), channel_id=5, replica_groups=mesh['sp'=8,'tp'=4] {'sp'}, dimensions={0}, use_global_device_ids=true | all-gather | bytes 18432 | tf_op jit(solution)/shard_map/all_gather | solution.py:11
  195.1 26.1 %all-gather.6 = f32[8,1,512]{2,1,0:T(1,128)S(1)} all-gather(f32[1,1,512]{2,1,0:T(1,128)S(1)} %bitcast.122), channel_id=4, replica_groups=mesh['sp'=8,'tp'=4] {'sp'}, dimensions={0}, use_global_device_ids=true | all-gather | bytes 18432 | tf_op jit(solution)/shard_map/all_gather | solution.py:11
  222.6 2.2 reshape.128
  224.9 2.2 reshape.129
  227.1 2.2 reshape.130
  229.3 2.2 multiply_add_fusion.1
  234.1 6.7 %all_to_all.10 = bf16[4,64,128]{2,1,0:T(8,128)(2,1)S(1)} all-to-all(bf16[4,64,128]{2,1,0:T(8,128)(2,1)S(1)} %fusion.45), channel_id=1, replica_groups=mesh['sp'=8,'tp'=4] {'tp'}, dimensions={0} | all-to-all | bytes 131072 | tf_op jit(solution)/shard_map/all_to_all | solution.py:145
  244.7 10.7 %all-gather.13.cloned.1.call-done = bf16[256,2048]{1,0:T(8,128)(2,1)} async-done(((bf16[64,2048]{1,0:T(8,128)(2,1)}), bf16[256,2048]{1,0:T(8,128)(2,1)}) %all-gather.13.cloned.1.call-update) | async-done | bytes 1048592 | tf_op jit(solution)/shard_map/all_gather | solution.py:157
  255.5 94.5 %all-gather.15.cloned.1.call-done = bf16[2048,1408]{1,0:T(8,128)(2,1)} async-done(((bf16[256,1408]{1,0:T(8,128)(2,1)}), bf16[2048,1408]{1,0:T(8,128)(2,1)}) %all-gather.15.cloned.1.call-update) | async-done | bytes 5767184 | tf_op jit(solution)/shard_map/all_gather | solution.py:160
  350.0 5.9 %fusion.57 = f32[256,1408]{1,0:T(8,128)} fusion(bf16[256,2048]{1,0:T(8,128)(2,1)} %all-gather.13.cloned.1.call-done, bf16[2048,1408]{1,0:T(8,128)(2,1)} %all-gather.15.cloned.1.call-done), kind=kOutput, calls=%fused_computation.104 | convolution fusion | flops 1476395008 | bytes 8257536 | tf_op jit(solution)/shard_map/dot_general | solution.py:158
  355.9 86.8 %all-gather.17.cloned.1.call-done = bf16[2048,1408]{1,0:T(8,128)(2,1)} async-done(((bf16[256,1408]{1,0:T(8,128)(2,1)}), bf16[2048,1408]{1,0:T(8,128)(2,1)}) %all-gather.17.cloned.1.call-update) | async-done | bytes 5767184 | tf_op jit(solution)/shard_map/all_gather | solution.py:164
  442.7 93.2 %all-gather.19.cloned.1.call-done = bf16[1408,2048]{1,0:T(8,128)(2,1)} async-done(((bf16[1408,256]{1,0:T(8,128)(2,1)}), bf16[1408,2048]{1,0:T(8,128)(2,1)}) %all-gather.19.cloned.1.call-update) | async-done | bytes 5767184 | tf_op jit(solution)/shard_map/all_gather | solution.py:168
  536.0 9.5 %convolution_convert_fusion = bf16[256,2048]{1,0:T(8,128)(2,1)} fusion(bf16[1408,2048]{1,0:T(8,128)(2,1)} %all-gather.19.cloned.1.call-done, bf16[256,2048]{1,0:T(8,128)(2,1)} %all-gather.13.cloned.1.call-done, bf16[2048,1408]{1,0:T(8,128)(2,1)} %all-gather.17.cloned.1.call-done, f32[256,1408]{1,0:T(8,128)} %fusion.57), kind=kOutput, calls=%fused_computation.53 | convolution fusion | flops 2955476992 | bytes 15073280 | tf_op jit(solution)/shard_map/dot_general | solution.py:167
  545.5 23.1 %reduce-scatter.2.cloned.1.call-done = bf16[64,2048]{1,0:T(8,128)(2,1)} async-done(((bf16[256,2048]{1,0:T(8,128)(2,1)}), bf16[64,2048]{1,0:T(8,128)(2,1)}) %reduce-scatter.2.cloned.1.call-update) | async-done | bytes 262160 | tf_op jit(solution)/shard_map/reduce_scatter | solution.py:170
  568.6 1.7 add_convert_fusion
  (140 shorter events, 33.3 us)
Async XLA Ops:
  6.5 234.4 %copy-start = (bf16[512,2048]{1,0:T(8,128)(2,1)S(1)}, bf16[512,2048]{1,0:T(8,128)(2,1)}, u32[]{:S(2)}) copy-start(bf16[512,2048]{1,0:T(8,128)(2,1)} %param.31) | copy-start | bytes 6291460
  6.5 8.8 %copy-start.2 = (f32[8,64,16]{1,2,0:T(8,128)S(1)}, f32[8,64,16]{1,2,0:T(8,128)}, u32[]{:S(2)}) copy-start(f32[8,64,16]{1,2,0:T(8,128)} %param.26) | copy-start | bytes 98308
  6.5 249.0 %all-gather.13.cloned.1.call-start = ((), (), s32[]{:S(2)}) async-start(), calls=%async_computation.2 | async-start | bytes 1310720 | tf_op jit(solution)/shard_map/all_gather | solution.py:157
  15.3 3.7 copy-start.6
  229.3 2.2 copy-start.3
  229.3 3.3 copy-start.4
  229.3 3.3 copy-start.7
  231.5 9.4 %copy-start.1 = (bf16[64,2048]{1,0:T(8,128)(2,1)S(1)}, bf16[64,2048]{1,0:T(8,128)(2,1)}, u32[]{:S(2)}) copy-start(bf16[64,2048]{1,0:T(8,128)(2,1)} %param.20) | copy-start | bytes 786436
  231.5 9.4 %copy-start.8 = (f32[512]{0:T(512)S(1)}, f32[512]{0:T(512)}, u32[]{:S(2)}) copy-start(f32[512]{0:T(512)} %param.30) | copy-start | bytes 6148
  233.8 7.8 %copy-start.5 = (f32[2048]{0:T(1024)S(1)}, f32[2048]{0:T(1024)}, u32[]{:S(2)}) copy-start(f32[2048]{0:T(1024)} %param.32) | copy-start | bytes 24580
  242.5 107.6 %all-gather.15.cloned.1.call-start = ((), (), s32[]{:S(2)}) async-start(), calls=%async_computation.3 | async-start | bytes 6488064 | tf_op jit(solution)/shard_map/all_gather | solution.py:160
  243.2 199.5 %all-gather.17.cloned.1.call-start = ((), (), s32[]{:S(2)}) async-start(), calls=%async_computation.4 | async-start | bytes 6488064 | tf_op jit(solution)/shard_map/all_gather | solution.py:164
  243.9 292.0 %all-gather.19.cloned.1.call-start = ((), (), s32[]{:S(2)}) async-start(), calls=%async_computation.5 | async-start | bytes 6488064 | tf_op jit(solution)/shard_map/all_gather | solution.py:168
  244.5 324.1 %reduce-scatter.2.cloned.1.call-start = ((), (), s32[]{:S(2)}) async-start(), calls=%async_computation.6 | async-start | bytes 1310720 | tf_op jit(solution)/shard_map/reduce_scatter | solution.py:170
Sparse Core Ops, SparseCore 0:
  242.6 12.8 all-gather.12
  257.7 92.3 all-gather.14
  352.2 90.4 all-gather.16
  444.6 91.2 all-gather.18
  545.6 22.9 reduce-scatter.1
where the time goes:
time: 578 us; the launch traced here: 577 us
  waiting for transfers between devices  310 us (54%)
  blocking collectives  113 us (20%)
  other arithmetic  90.7 us (16%)
  local copies, waits for them, and re-layouts  25.5 us (4%)
  matrix products  23.1 us (4%)
  between operations  13.3 us (2%)
    all_gather x4, blocking collectives, carried_in(): gathered = jax.tree.map(lambda a: lax.all_gather(a, axis), part)  106 us
    all_gather x1, waiting for transfers between devices, per_device(): lax.all_gather(gating_matrix, 'sp', axis=0, tiled=True)  94.5 us
    all_gather x1, waiting for transfers between devices, per_device(): lax.all_gather(w_down, 'sp', axis=1, tiled=True)  93.2 us
    all_gather x1, waiting for transfers between devices, per_device(): lax.all_gather(w_up, 'sp', axis=0, tiled=True)  86.8 us
    reduce_sum x8, other arithmetic, advance(): jnp.sum(weight_real * imag_block[None] + weight_imag * real_block[None],...  73.6 us
    reduce_scatter x1, waiting for transfers between devices, per_device(): lax.psum_scatter(partial_value.astype(jnp.bfloat16), 'tp', scatter_dimens...  23.1 us
  transfers between devices with their start and end apart: 5, of which 5 were waited for; matrix products, arithmetic and copies ran while one was open for 1% of the time, Pallas kernels for 0%

commit v1 on v0

--- a/solution.py
+++ b/solution.py
@@ -2,6 +2,7 @@
 import jax.numpy as jnp
 from jax import lax
 from jax.sharding import PartitionSpec as P
+from jax.lax import all_gather
 
 eps = 1e-06
 
@@ -164,9 +165,10 @@
         gathered, lax.all_gather(w_up, "sp", axis=0, tiled=True), preferred_element_type=jnp.float32
     )
     hidden = (jax.nn.silu(gate_val) * up_val).astype(jnp.bfloat16)
-    partial_value = jnp.dot(
-        hidden, lax.all_gather(w_down, "sp", axis=1, tiled=True), preferred_element_type=jnp.float32
+    steps_all_find = lambda local_values: jnp.concatenate(
+        all_gather(local_values, axis_name="sp"), 1
     )
+    partial_value = jnp.dot(hidden, steps_all_find(w_down), preferred_element_type=jnp.float32)
     ffn = lax.psum_scatter(
         partial_value.astype(jnp.bfloat16), "tp", scatter_dimension=0, tiled=True
     ).astype(jnp.float32)

time: 578 us -> 486 us (0.84)
  waiting for transfers between devices: 310 us -> 209 us
  local copies, waits for them, and re-layouts: 25.5 us -> 34 us
    all_gather x1, waiting for transfers between devices: 93.2 us -> 0.02 us  [per_device(): all_gather(local_values, axis_name='sp')]
    reshape x0 -> x1, local copies, waits for them, and re-layouts: none -> 8.4 us  [per_device(): jnp.concatenate(all_gather(local_values, axis_name='sp'), 1)]
    all_gather x1, waiting for transfers between devices: 10.7 us -> 3.06 us  [per_device(): gathered = lax.all_gather(ffn_in, 'tp', axis=0, tiled=True)]
  transfers between devices with their start and end apart: 5 -> 5, of which waited for: 5 -> 4; matrix products, arithmetic and copies ran while one was open for 1% -> 28% of each run, Pallas kernels for 0% -> 0%
where the time goes in v1:
time: 486 us; the launch traced here: 484 us
  waiting for transfers between devices  209 us (43%)
  blocking collectives  113 us (23%)
  other arithmetic  90.6 us (19%)
  local copies, waits for them, and re-layouts  34 us (7%)
  matrix products  23.2 us (5%)
  between operations  13.4 us (3%)
    all_gather x4, blocking collectives, carried_in(): gathered = jax.tree.map(lambda a: lax.all_gather(a, axis), part)  106 us
    all_gather x1, waiting for transfers between devices, per_device(): lax.all_gather(gating_matrix, 'sp', axis=0, tiled=True)  94.5 us
    all_gather x1, waiting for transfers between devices, per_device(): lax.all_gather(w_up, 'sp', axis=0, tiled=True)  86.7 us
    reduce_sum x8, other arithmetic, advance(): jnp.sum(weight_real * imag_block[None] + weight_imag * real_block[None],...  73.6 us
    reduce_scatter x1, waiting for transfers between devices, per_device(): lax.psum_scatter(partial_value.astype(jnp.bfloat16), 'tp', scatter_dimens...  23.1 us
    dynamic_update_slice x8, other arithmetic, local_states(): final, outputs = lax.scan(advance, start, blocks)  9.94 us
  transfers between devices with their start and end apart: 5, of which 4 were waited for; matrix products, arithmetic and copies ran while one was open for 28% of the time, Pallas kernels for 0%

profile of v1, /device:TPU:0, one launch (start us, length us, event | category | flops | bytes accessed | tf_op | source)
XLA Modules:
  0.0 484.3 jit_solution(6662259509079659011)
XLA Ops:
  11.3 2.1 convolution_bitcast_fusion.2
  13.4 1.5 copy.62
  17.2 1.5 copy.63
  22.5 93.2 %while.45 = (s32[]{:T(128)}, f32[512]{0:T(512)S(1)}, f32[512]{0:T(512)S(1)}, f32[512]{0:T(512)S(1)}, f32[]{:T(128)}, /*index=5*/f32[8,32,512]{2,1,0:T(8,128)}, f...) while((s32[]{:T(128)}, f32[512]{0:T(512)S(1)}, ...), condition=%wide.wide.region_3.4_spmd.clone.clone.clone.clone, body=%wide.wide.region_0.3_spmd.clone.clone.clone.clone.sunk | while | flops 14897220 | bytes 1351775 | solution.py:79
  23.6 9.2 %add_reduce_fusion.3 = (f32[32,512]{1,0:T(8,128)S(1)}, f32[32,512]{1,0:T(8,128)S(1)}) fusion(f32[512]{0:T(512)S(1)} %get-tuple-element.853, f32[32,32]{1,0:T(8,128)S(1)} %get-tuple-element.854, f32[32,512]{1,0:T(8,128)S(1)} %get-tuple-element.788, f32[32,512]{1,0:T(8,128)S(1)} %get-tuple-element.789, ...), kind=kLoop, calls=%fused_computation.19.clone.clone.1 | loop fusion | flops 8355840 | bytes 335872 | tf_op jit(solution)/shard_map/while/body/eval_jaxpr/reduce_sum | solution.py:59
  32.9 1.2 fusion.82
  35.3 9.2 %add_reduce_fusion.3 = (f32[32,512]{1,0:T(8,128)S(1)}, f32[32,512]{1,0:T(8,128)S(1)}) fusion(f32[512]{0:T(512)S(1)} %get-tuple-element.853, f32[32,32]{1,0:T(8,128)S(1)} %get-tuple-element.854, f32[32,512]{1,0:T(8,128)S(1)} %get-tuple-element.788, f32[32,512]{1,0:T(8,128)S(1)} %get-tuple-element.789, ...), kind=kLoop, calls=%fused_computation.19.clone.clone.1 | loop fusion | flops 8355840 | bytes 335872 | tf_op jit(solution)/shard_map/while/body/eval_jaxpr/reduce_sum | solution.py:59
  46.9 9.2 %add_reduce_fusion.3 = (f32[32,512]{1,0:T(8,128)S(1)}, f32[32,512]{1,0:T(8,128)S(1)}) fusion(f32[512]{0:T(512)S(1)} %get-tuple-element.853, f32[32,32]{1,0:T(8,128)S(1)} %get-tuple-element.854, f32[32,512]{1,0:T(8,128)S(1)} %get-tuple-element.788, f32[32,512]{1,0:T(8,128)S(1)} %get-tuple-element.789, ...), kind=kLoop, calls=%fused_computation.19.clone.clone.1 | loop fusion | flops 8355840 | bytes 335872 | tf_op jit(solution)/shard_map/while/body/eval_jaxpr/reduce_sum | solution.py:59
  58.6 9.2 %add_reduce_fusion.3 = (f32[32,512]{1,0:T(8,128)S(1)}, f32[32,512]{1,0:T(8,128)S(1)}) fusion(f32[512]{0:T(512)S(1)} %get-tuple-element.853, f32[32,32]{1,0:T(8,128)S(1)} %get-tuple-element.854, f32[32,512]{1,0:T(8,128)S(1)} %get-tuple-element.788, f32[32,512]{1,0:T(8,128)S(1)} %get-tuple-element.789, ...), kind=kLoop, calls=%fused_computation.19.clone.clone.1 | loop fusion | flops 8355840 | bytes 335872 | tf_op jit(solution)/shard_map/while/body/eval_jaxpr/reduce_sum | solution.py:59
  67.8 1.2 fusion.82
  70.2 9.2 %add_reduce_fusion.3 = (f32[32,512]{1,0:T(8,128)S(1)}, f32[32,512]{1,0:T(8,128)S(1)}) fusion(f32[512]{0:T(512)S(1)} %get-tuple-element.853, f32[32,32]{1,0:T(8,128)S(1)} %get-tuple-element.854, f32[32,512]{1,0:T(8,128)S(1)} %get-tuple-element.788, f32[32,512]{1,0:T(8,128)S(1)} %get-tuple-element.789, ...), kind=kLoop, calls=%fused_computation.19.clone.clone.1 | loop fusion | flops 8355840 | bytes 335872 | tf_op jit(solution)/shard_map/while/body/eval_jaxpr/reduce_sum | solution.py:59
  81.9 9.2 %add_reduce_fusion.3 = (f32[32,512]{1,0:T(8,128)S(1)}, f32[32,512]{1,0:T(8,128)S(1)}) fusion(f32[512]{0:T(512)S(1)} %get-tuple-element.853, f32[32,32]{1,0:T(8,128)S(1)} %get-tuple-element.854, f32[32,512]{1,0:T(8,128)S(1)} %get-tuple-element.788, f32[32,512]{1,0:T(8,128)S(1)} %get-tuple-element.789, ...), kind=kLoop, calls=%fused_computation.19.clone.clone.1 | loop fusion | flops 8355840 | bytes 335872 | tf_op jit(solution)/shard_map/while/body/eval_jaxpr/reduce_sum | solution.py:59
  93.5 9.2 %add_reduce_fusion.3 = (f32[32,512]{1,0:T(8,128)S(1)}, f32[32,512]{1,0:T(8,128)S(1)}) fusion(f32[512]{0:T(512)S(1)} %get-tuple-element.853, f32[32,32]{1,0:T(8,128)S(1)} %get-tuple-element.854, f32[32,512]{1,0:T(8,128)S(1)} %get-tuple-element.788, f32[32,512]{1,0:T(8,128)S(1)} %get-tuple-element.789, ...), kind=kLoop, calls=%fused_computation.19.clone.clone.1 | loop fusion | flops 8355840 | bytes 335872 | tf_op jit(solution)/shard_map/while/body/eval_jaxpr/reduce_sum | solution.py:59
  105.2 9.2 %add_reduce_fusion.3 = (f32[32,512]{1,0:T(8,128)S(1)}, f32[32,512]{1,0:T(8,128)S(1)}) fusion(f32[512]{0:T(512)S(1)} %get-tuple-element.853, f32[32,32]{1,0:T(8,128)S(1)} %get-tuple-element.854, f32[32,512]{1,0:T(8,128)S(1)} %get-tuple-element.788, f32[32,512]{1,0:T(8,128)S(1)} %get-tuple-element.789, ...), kind=kLoop, calls=%fused_computation.19.clone.clone.1 | loop fusion | flops 8355840 | bytes 335872 | tf_op jit(solution)/shard_map/while/body/eval_jaxpr/reduce_sum | solution.py:59
  114.4 1.2 fusion.82
  115.7 27.9 %all-gather.6 = f32[8,1,512]{2,1,0:T(1,128)S(1)} all-gather(f32[1,1,512]{2,1,0:T(1,128)S(1)} %bitcast.136), channel_id=3, replica_groups=mesh['sp'=8,'tp'=4] {'sp'}, dimensions={0}, use_global_device_ids=true | all-gather | bytes 18432 | tf_op jit(solution)/shard_map/all_gather | solution.py:12
  143.7 26.1 %all-gather.5 = f32[8,1,512]{2,1,0:T(1,128)S(1)} all-gather(f32[1,1,512]{2,1,0:T(1,128)S(1)} %bitcast.135), channel_id=2, replica_groups=mesh['sp'=8,'tp'=4] {'sp'}, dimensions={0}, use_global_device_ids=true | all-gather | bytes 18432 | tf_op jit(solution)/shard_map/all_gather | solution.py:12
  169.8 26.1 %all-gather.8 = f32[8,1,512]{2,1,0:T(1,128)S(1)} all-gather(f32[1,1,512]{2,1,0:T(1,128)S(1)} %bitcast.130), channel_id=5, replica_groups=mesh['sp'=8,'tp'=4] {'sp'}, dimensions={0}, use_global_device_ids=true | all-gather | bytes 18432 | tf_op jit(solution)/shard_map/all_gather | solution.py:12
  195.9 26.1 %all-gather.7 = f32[8,1,512]{2,1,0:T(1,128)S(1)} all-gather(f32[1,1,512]{2,1,0:T(1,128)S(1)} %bitcast.128), channel_id=4, replica_groups=mesh['sp'=8,'tp'=4] {'sp'}, dimensions={0}, use_global_device_ids=true | all-gather | bytes 18432 | tf_op jit(solution)/shard_map/all_gather | solution.py:12
  223.4 2.2 reshape.134
  225.7 2.2 reshape.135
  227.9 2.3 reshape.136
  230.2 2.2 multiply_add_fusion.1
  235.0 6.7 %all_to_all.10 = bf16[4,64,128]{2,1,0:T(8,128)(2,1)S(1)} all-to-all(bf16[4,64,128]{2,1,0:T(8,128)(2,1)S(1)} %fusion.45), channel_id=1, replica_groups=mesh['sp'=8,'tp'=4] {'tp'}, dimensions={0} | all-to-all | bytes 131072 | tf_op jit(solution)/shard_map/all_to_all | solution.py:146
  244.9 8.4 %copy.72 = bf16[1408,8,256]{0,2,1:T(8,128)(2,1)} copy(bf16[1408,8,256]{2,0,1:T(8,128)(2,1)} %bitcast.117) | data formatting | bytes 11534336 | tf_op jit(solution)/shard_map/reshape | solution.py:168
  253.3 3.1 all-gather.14.cloned.1.call-done
  256.3 94.5 %all-gather.16.cloned.1.call-done = bf16[2048,1408]{1,0:T(8,128)(2,1)} async-done(((bf16[256,1408]{1,0:T(8,128)(2,1)}), bf16[2048,1408]{1,0:T(8,128)(2,1)}) %all-gather.16.cloned.1.call-update) | async-done | bytes 5767184 | tf_op jit(solution)/shard_map/all_gather | solution.py:161
  350.9 5.9 %fusion.57 = f32[256,1408]{1,0:T(8,128)} fusion(bf16[256,2048]{1,0:T(8,128)(2,1)} %all-gather.14.cloned.1.call-done, bf16[2048,1408]{1,0:T(8,128)(2,1)} %all-gather.16.cloned.1.call-done), kind=kOutput, calls=%fused_computation.104 | convolution fusion | flops 1476395008 | bytes 8257536 | tf_op jit(solution)/shard_map/dot_general | solution.py:159
  356.8 86.7 %all-gather.18.cloned.1.call-done = bf16[2048,1408]{1,0:T(8,128)(2,1)} async-done(((bf16[256,1408]{1,0:T(8,128)(2,1)}), bf16[2048,1408]{1,0:T(8,128)(2,1)}) %all-gather.18.cloned.1.call-update) | async-done | bytes 5767184 | tf_op jit(solution)/shard_map/all_gather | solution.py:165
  443.4 9.5 %convolution_convert_fusion = bf16[256,2048]{1,0:T(8,128)(2,1)} fusion(bf16[1408,2048]{0,1:T(8,128)(2,1)} %bitcast.118, bf16[256,2048]{1,0:T(8,128)(2,1)} %all-gather.14.cloned.1.call-done, bf16[2048,1408]{1,0:T(8,128)(2,1)} %all-gather.18.cloned.1.call-done, f32[256,1408]{1,0:T(8,128)} %fusion.57), kind=kOutput, calls=%fused_computation.53 | convolution fusion | flops 2955476992 | bytes 15073280 | tf_op jit(solution)/shard_map/dot_general | solution.py:171
  452.9 23.1 %reduce-scatter.2.cloned.1.call-done = bf16[64,2048]{1,0:T(8,128)(2,1)} async-done(((bf16[256,2048]{1,0:T(8,128)(2,1)}), bf16[64,2048]{1,0:T(8,128)(2,1)}) %reduce-scatter.2.cloned.1.call-update) | async-done | bytes 262160 | tf_op jit(solution)/shard_map/reduce_scatter | solution.py:172
  476.1 1.7 add_convert_fusion
  (141 shorter events, 33.3 us)
Async XLA Ops:
  6.5 235.2 %copy-start = (bf16[512,2048]{1,0:T(8,128)(2,1)S(1)}, bf16[512,2048]{1,0:T(8,128)(2,1)}, u32[]{:S(2)}) copy-start(bf16[512,2048]{1,0:T(8,128)(2,1)} %param.31) | copy-start | bytes 6291460
  6.5 238.3 %all-gather.20.cloned.1.call-start = ((), (), s32[]{:S(2)}) async-start(), calls=%async_computation.6 | async-start | bytes 6488064 | tf_op jit(solution)/shard_map/all_gather | solution.py:169
  7.3 8.7 %copy-start.2 = (f32[8,64,16]{1,2,0:T(8,128)S(1)}, f32[8,64,16]{1,2,0:T(8,128)}, u32[]{:S(2)}) copy-start(f32[8,64,16]{1,2,0:T(8,128)} %param.26) | copy-start | bytes 98308
  7.3 249.1 %all-gather.14.cloned.1.call-start = ((), (), s32[]{:S(2)}) async-start(), calls=%async_computation.2 | async-start | bytes 1310720 | tf_op jit(solution)/shard_map/all_gather | solution.py:158
  16.0 3.7 copy-start.6
  230.2 2.2 copy-start.3
  230.2 3.3 copy-start.4
  230.2 3.3 copy-start.7
  232.3 9.4 %copy-start.1 = (bf16[64,2048]{1,0:T(8,128)(2,1)S(1)}, bf16[64,2048]{1,0:T(8,128)(2,1)}, u32[]{:S(2)}) copy-start(bf16[64,2048]{1,0:T(8,128)(2,1)} %param.20) | copy-start | bytes 786436
  232.4 9.4 %copy-start.8 = (f32[512]{0:T(512)S(1)}, f32[512]{0:T(512)}, u32[]{:S(2)}) copy-start(f32[512]{0:T(512)} %param.30) | copy-start | bytes 6148
  234.6 7.8 %copy-start.5 = (f32[2048]{0:T(1024)S(1)}, f32[2048]{0:T(1024)}, u32[]{:S(2)}) copy-start(f32[2048]{0:T(1024)} %param.32) | copy-start | bytes 24580
  243.3 107.6 %all-gather.16.cloned.1.call-start = ((), (), s32[]{:S(2)}) async-start(), calls=%async_computation.3 | async-start | bytes 6488064 | tf_op jit(solution)/shard_map/all_gather | solution.py:161
  244.0 199.4 %all-gather.18.cloned.1.call-start = ((), (), s32[]{:S(2)}) async-start(), calls=%async_computation.4 | async-start | bytes 6488064 | tf_op jit(solution)/shard_map/all_gather | solution.py:165
  244.6 231.4 %reduce-scatter.2.cloned.1.call-start = ((), (), s32[]{:S(2)}) async-start(), calls=%async_computation.5 | async-start | bytes 1310720 | tf_op jit(solution)/shard_map/reduce_scatter | solution.py:172
Sparse Core Ops, SparseCore 0:
  9.5 95.0 all-gather.19
  243.4 12.8 all-gather.13
  258.5 92.3 all-gather.15
  352.9 90.4 all-gather.17
  453.1 22.9 reduce-scatter.1
